TPU v7x, 32 devices: a whole 2x2x4 slice. The times are simulated.
32 devices in a mesh: rep: 2 (over x), fs: 4 (over z), tp: 4 (over y, core).
Axes of the slice: x: 2, y: 2, z: 4, core: 2. Of those that a mesh axis runs over, the one named last changes fastest.
Arguments:
- tokens: bfloat16 [8192, 2048], P(('rep', 'fs'), 'tp'), may hold values from -6 to 6
- mix_gain: float32 [2048], replicated, may hold values from 0.1 to 1.9
- query_weight: bfloat16 [2048, 512], P('fs', 'tp'), may hold values from -0.125 to 0.125
- key_weight: bfloat16 [2048, 512], P('fs', 'tp'), may hold values from -0.125 to 0.125
- value_weight: bfloat16 [2048, 1024], P('fs', 'tp'), may hold values from -0.125 to 0.125
- gate_weight: bfloat16 [2048, 1024], P('fs', 'tp'), may hold values from -0.125 to 0.125
- out_weight: bfloat16 [1024, 2048], P('tp', 'fs'), may hold values from -0.1875 to 0.1875
- head_gain: float32 [8, 128], P('tp'), may hold values from 0.1 to 1.9
- ffn_gain: float32 [2048], replicated, may hold values from 0.1 to 1.9
- ffn_gate: bfloat16 [2048, 5632], P('fs', 'tp'), may hold values from -0.125 to 0.125
- ffn_up: bfloat16 [2048, 5632], P('fs', 'tp'), may hold values from -0.125 to 0.125
- ffn_down: bfloat16 [5632, 2048], P('tp', 'fs'), may hold values from -0.078125 to 0.078125
Outputs:
- layer_out: bfloat16 [8192, 2048], P(('rep', 'fs'), 'tp')
All inputs are finite; a program needn't handle non-finite values.
Results may differ from a plain program's by a relative error of at most 0.03.
Values may be sent and summed in bfloat16 or wider, within the bound.
A program may use at most 128 MiB of HBM per device.

v0:
```python
import jax
import jax.numpy as jnp
from jax import lax
from jax.sharding import PartitionSpec as P

HEADS = 8
DK = 64
DV = 128
BLOCK = 64
SEQ = 256
epsilon = 1e-06
rope_base = 10000.0


def norm_rows(values, gain_row):
    floats = values.astype(jnp.float32)
    scaled = floats * lax.rsqrt(jnp.mean(floats * floats, axis=-1, keepdims=True) + epsilon)
    return (scaled * gain_row).astype(jnp.bfloat16)


def rotate(values, positions):
    half_dim = values.shape[-1] // 2
    frequency = rope_base ** (-jnp.linspace(0.0, 1.0, half_dim, dtype=jnp.float32))
    angles = positions.astype(jnp.float32)[:, None] * frequency[None, :]
    cosine = jnp.cos(angles)[:, None, :]
    sine_part = jnp.sin(angles)[:, None, :]
    paired = values.reshape(values.shape[:-1] + (half_dim, 2))
    leading = paired[..., 0]
    trailing = paired[..., 1]
    turned = jnp.stack(
        [leading * cosine - trailing * sine_part, leading * sine_part + trailing * cosine], axis=-1
    )
    return turned.reshape(values.shape)


def log_decay(head_index, total_heads):
    return jnp.log1p(-jnp.exp2(-5.0 - 4.0 * head_index.astype(jnp.float32) / (total_heads - 1)))


def retention(queries, key_rows, value_rows, decay_rates):
    highest = lax.Precision.HIGHEST
    row_count, head_count = (queries.shape[0], queries.shape[1])
    seq_count = row_count // SEQ
    block_count = SEQ // BLOCK

    def to_blocks(values):
        shaped = values.reshape((seq_count, block_count, BLOCK) + values.shape[1:])
        return jnp.moveaxis(shaped, 1, 0)

    inside = jnp.arange(BLOCK, dtype=jnp.int32)
    gap = (inside[:, None] - inside[None, :]).astype(jnp.float32)
    within_mask = jnp.where(
        gap[None] >= 0.0, jnp.exp(jnp.maximum(gap, 0.0)[None] * decay_rates[:, None, None]), 0.0
    )
    query_scale = jnp.exp((inside + 1).astype(jnp.float32)[:, None] * decay_rates[None, :])
    key_scale = jnp.exp((BLOCK - 1 - inside).astype(jnp.float32)[:, None] * decay_rates[None, :])
    block_decay = jnp.exp(BLOCK * decay_rates)

    def advance(state, inputs):
        query_blk, key_blk, value_blk = inputs
        scores = (
            jnp.einsum("sihd,sjhd->shij", query_blk, key_blk, precision=highest) * within_mask[None]
        )
        local_part = jnp.einsum("shij,sjhv->sihv", scores, value_blk, precision=highest)
        carried = jnp.einsum(
            "sihd,shdv->sihv", query_blk * query_scale[None, :, :, None], state, precision=highest
        )
        update = jnp.einsum(
            "sjhd,sjhv->shdv", key_blk * key_scale[None, :, :, None], value_blk, precision=highest
        )
        return (block_decay[None, :, None, None] * state + update, local_part + carried)

    state_zero = jnp.zeros((seq_count, head_count, DK, DV), jnp.float32)
    _, outputs = lax.scan(
        advance, state_zero, (to_blocks(queries), to_blocks(key_rows), to_blocks(value_rows))
    )
    return jnp.moveaxis(outputs, 0, 1).reshape(row_count, head_count, DV)


def per_device(
    tokens,
    mix_gain,
    query_weight,
    key_weight,
    value_weight,
    gate_weight,
    out_weight,
    head_gain,
    ffn_gain,
    ffn_gate,
    ffn_up,
    ffn_down,
):
    whole_rows = lax.all_gather(tokens, "tp", axis=1, tiled=True)
    row_count = whole_rows.shape[0]
    normed = norm_rows(whole_rows, mix_gain)
    pieces = (
        lax.all_gather(query_weight, "fs", axis=0, tiled=True),
        lax.all_gather(key_weight, "fs", axis=0, tiled=True),
        lax.all_gather(value_weight, "fs", axis=0, tiled=True),
        lax.all_gather(gate_weight, "fs", axis=0, tiled=True),
    )
    query_acc, key_acc, value_acc, gate_acc = tuple(
        (
            jnp.dot(normed, weight_piece, preferred_element_type=jnp.float32)
            for weight_piece in pieces
        )
    )
    heads_here = query_weight.shape[1] // DK
    positions = jnp.arange(row_count, dtype=jnp.int32) % SEQ
    queries = rotate(
        query_acc.astype(jnp.bfloat16).astype(jnp.float32).reshape(row_count, heads_here, DK),
        positions,
    )
    key_rows = rotate(
        key_acc.astype(jnp.bfloat16).astype(jnp.float32).reshape(row_count, heads_here, DK),
        positions,
    ) * DK ** (-0.5)
    value_rows = (
        value_acc.astype(jnp.bfloat16).astype(jnp.float32).reshape(row_count, heads_here, DV)
    )
    gate_rows = gate_acc.astype(jnp.bfloat16).astype(jnp.float32)
    first_head = lax.axis_index("tp") * heads_here
    decay_rates = log_decay(first_head + jnp.arange(heads_here, dtype=jnp.int32), HEADS)
    retained = retention(queries, key_rows, value_rows, decay_rates)
    center = jnp.mean(retained, axis=-1, keepdims=True)
    spread = jnp.mean(jnp.square(retained - center), axis=-1, keepdims=True)
    grouped = (retained - center) * lax.rsqrt(spread + epsilon) * head_gain[None]
    mixed = (grouped.reshape(row_count, heads_here * DV) * jax.nn.silu(gate_rows)).astype(
        jnp.bfloat16
    )
    mixer_terms = jnp.dot(
        mixed,
        lax.all_gather(out_weight, "fs", axis=1, tiled=True),
        preferred_element_type=jnp.float32,
    )
    mixer_share = lax.psum_scatter(
        mixer_terms.astype(jnp.bfloat16), "tp", scatter_dimension=1, tiled=True
    ).astype(jnp.float32)
    resid_shard = (tokens.astype(jnp.float32) + mixer_share).astype(jnp.bfloat16)
    resid_whole = lax.all_gather(resid_shard, "tp", axis=1, tiled=True)
    normed_ffn = norm_rows(resid_whole, ffn_gain)

    def add_rows(weight_piece):
        return jnp.dot(normed_ffn, weight_piece, preferred_element_type=jnp.float32)

    gate_hidden = add_rows(lax.all_gather(ffn_gate, "fs", axis=0, tiled=True))
    up_hidden = add_rows(lax.all_gather(ffn_up, "fs", axis=0, tiled=True))
    hidden = (jax.nn.silu(gate_hidden) * up_hidden).astype(jnp.bfloat16)
    ffn_terms = jnp.dot(
        hidden,
        lax.all_gather(ffn_down, "fs", axis=1, tiled=True),
        preferred_element_type=jnp.float32,
    )
    ffn_share = lax.psum_scatter(
        ffn_terms.astype(jnp.bfloat16), "tp", scatter_dimension=1, tiled=True
    ).astype(jnp.float32)
    return (resid_shard.astype(jnp.float32) + ffn_share).astype(jnp.bfloat16)


def solution(mesh):
    return jax.shard_map(
        per_device,
        mesh=mesh,
        in_specs=(
            P(("rep", "fs"), "tp"),
            P(),
            P("fs", "tp"),
            P("fs", "tp"),
            P("fs", "tp"),
            P("fs", "tp"),
            P("tp", "fs"),
            P("tp", None),
            P(),
            P("fs", "tp"),
            P("fs", "tp"),
            P("tp", "fs"),
        ),
        out_specs=P(("rep", "fs"), "tp"),
        check_vma=False,
    )
```

profile of v0, /device:TPU:0, one launch (start us, length us, event | category | flops | bytes accessed | tf_op | source)
XLA Modules:
  0.0 622.1 jit_solution(10062320432352257111)
XLA Ops:
  9.5 17.6 %all_gather.31 = bf16[2048,128]{1,0:T(8,128)(2,1)S(1)} all-gather(bf16[512,128]{1,0:T(8,128)(2,1)} %param.19), channel_id=1, replica_groups=mesh['rep'=2,'fs'=4,'tp'=4] {'fs'}, dimensions={0}, use_global_device_ids=true | all-gather | bytes 655360 | tf_op jit(solution)/shard_map/all_gather | solution.py:99
  27.0 16.6 %all_gather.33 = bf16[2048,128]{1,0:T(8,128)(2,1)S(1)} all-gather(bf16[512,128]{1,0:T(8,128)(2,1)} %param.18), channel_id=1, replica_groups=mesh['rep'=2,'fs'=4,'tp'=4] {'fs'}, dimensions={0}, use_global_device_ids=true | all-gather | bytes 655360 | tf_op jit(solution)/shard_map/all_gather | solution.py:98
  46.1 3.2 fusion.25
  50.6 1.9 copy-done
  52.5 1.5 fusion.36
  54.4 3.9 fusion.35
  58.5 2.1 multiply_subtract_fusion
  61.6 1.8 mul.286
  63.4 1.9 reshape_reshape.24
  65.3 10.4 %all-gather.11.cloned.1.call-done = bf16[2048,256]{1,0:T(8,128)(2,1)} async-done(((bf16[512,256]{1,0:T(8,128)(2,1)}), bf16[2048,256]{1,0:T(8,128)(2,1)}) %all-gather.11.cloned.1.call-update) | async-done | bytes 1048592 | tf_op jit(solution)/shard_map/all_gather | solution.py:100
  75.7 3.7 fusion.31
  80.1 19.0 %while.15 = (s32[]{:T(128)}, f32[4,2,64,128]{3,2,1,0:T(8,128)S(1)}, f32[4,4,64,2,128]{4,2,3,1,0:T(8,128)S(1)}, f32[4,4,64,2,64]{2,0,1,4,3:T(4,128)}, f32[4,4,64,...) while((s32[]{:T(128)}, f32[4,2,64,128]{3,2,1,0:T(8,128)S(1)}, ...), condition=%wide.region_2.4_spmd.clone.clone.clone, body=%wide.region_1.3_spmd.clone.clone.clone.sunk | while | flops 176603408 | bytes 4415676 | solution.py:74
  80.3 2.1 constant_dynamic-slice_fusion.3
  85.0 2.1 constant_dynamic-slice_fusion.3
  89.7 2.1 constant_dynamic-slice_fusion.3
  94.4 2.1 constant_dynamic-slice_fusion.3
  100.7 1.8 copy.35
  102.5 2.2 all-gather.13.cloned.1.call-done
  104.7 28.8 %all-gather.15.cloned.1.call-done = bf16[256,2048]{1,0:T(8,128)(2,1)} async-done(((bf16[256,512]{1,0:T(8,128)(2,1)}), bf16[256,2048]{1,0:T(8,128)(2,1)}) %all-gather.15.cloned.1.call-update) | async-done | bytes 1048592 | tf_op jit(solution)/shard_map/all_gather | solution.py:134
  134.7 2.0 sub.86
  136.8 9.9 %convolution_convert_fusion.1 = bf16[1024,2048]{1,0:T(8,128)(2,1)} fusion(bf16[256,2048]{1,0:T(8,128)(2,1)} %all-gather.15.cloned.1.call-done, bf16[1024,2048]{1,0:T(8,128)(2,1)} %copy-done, bf16[2048,256]{1,0:T(8,128)(2,1)} %all-gather.13.cloned.1.call-done, f32[128,8,2,128]{3,2,1,0:T(2,128)S(1)} %bitcast.114, f32[128,8,2,128]{3,2,1,0:T(2,128)} %bitcast.115, ...), kind=kOutput, calls=%fused_computation.45 | convolution fusion | flops 2152464384 | bytes 13632512 | tf_op jit(solution)/shard_map/dot_general | solution.py:132
  146.8 43.9 %reduce-scatter.3.cloned.1.call-done = bf16[1024,512]{1,0:T(8,128)(2,1)} async-done(((bf16[1024,2048]{1,0:T(8,128)(2,1)}), bf16[1024,512]{1,0:T(8,128)(2,1)}) %reduce-scatter.3.cloned.1.call-update) | async-done | bytes 1048592 | tf_op jit(solution)/shard_map/reduce_scatter | solution.py:137
  190.6 2.5 add_convert_fusion.1
  195.4 32.3 %all-gather.17.cloned.1.call-done = bf16[1024,2048]{1,0:T(8,128)(2,1)} async-done(((bf16[1024,512]{1,0:T(8,128)(2,1)}), bf16[1024,2048]{1,0:T(8,128)(2,1)}) %all-gather.17.cloned.1.call-update) | async-done | bytes 4194320 | tf_op jit(solution)/shard_map/all_gather | solution.py:141
  227.7 3.1 fusion.28
  230.8 105.2 %all-gather.19.cloned.1.call-done = bf16[2048,1408]{1,0:T(8,128)(2,1)} async-done(((bf16[512,1408]{1,0:T(8,128)(2,1)}), bf16[2048,1408]{1,0:T(8,128)(2,1)}) %all-gather.19.cloned.1.call-update) | async-done | bytes 5767184 | tf_op jit(solution)/shard_map/all_gather | solution.py:147
  336.0 11.9 %fusion.33 = f32[1024,1408]{1,0:T(8,128)} fusion(bf16[2048,1408]{1,0:T(8,128)(2,1)} %all-gather.19.cloned.1.call-done, bf16[1024,2048]{1,0:T(8,128)(2,1)} %all-gather.17.cloned.1.call-done, f32[2048]{0:T(1024)S(1)} %copy-done.5, f32[1024]{0:T(1024)S(1)} %add_rsqrt_fusion), kind=kOutput, calls=%fused_computation.53 | convolution fusion | flops 5913968640 | bytes 15740928 | tf_op jit(solution)/shard_map/dot_general | solution.py:145
  347.9 94.7 %all-gather.21.cloned.1.call-done = bf16[2048,1408]{1,0:T(8,128)(2,1)} async-done(((bf16[512,1408]{1,0:T(8,128)(2,1)}), bf16[2048,1408]{1,0:T(8,128)(2,1)}) %all-gather.21.cloned.1.call-update) | async-done | bytes 5767184 | tf_op jit(solution)/shard_map/all_gather | solution.py:148
  442.6 106.5 %all-gather.23.cloned.1.call-done = bf16[1408,2048]{1,0:T(8,128)(2,1)} async-done(((bf16[1408,512]{1,0:T(8,128)(2,1)}), bf16[1408,2048]{1,0:T(8,128)(2,1)}) %all-gather.23.cloned.1.call-update) | async-done | bytes 5767184 | tf_op jit(solution)/shard_map/all_gather | solution.py:152
  549.1 20.9 %convolution_convert_fusion = bf16[1024,2048]{1,0:T(8,128)(2,1)} fusion(bf16[1408,2048]{1,0:T(8,128)(2,1)} %all-gather.23.cloned.1.call-done, f32[1024,1408]{1,0:T(8,128)} %fusion.33, bf16[2048,1408]{1,0:T(8,128)(2,1)} %all-gather.21.cloned.1.call-done, bf16[1024,2048]{1,0:T(8,128)(2,1)} %all-gather.17.cloned.1.call-done, f32[2048]{0:T(1024)S(1)} %copy-done.5, ...), kind=kOutput, calls=%fused_computation.44 | convolution fusion | flops 11830296576 | bytes 25702400 | tf_op jit(solution)/shard_map/dot_general | solution.py:150
  570.0 42.8 %reduce-scatter.5.cloned.1.call-done = bf16[1024,512]{1,0:T(8,128)(2,1)} async-done(((bf16[1024,2048]{1,0:T(8,128)(2,1)}), bf16[1024,512]{1,0:T(8,128)(2,1)}) %reduce-scatter.5.cloned.1.call-update) | async-done | bytes 1048592 | tf_op jit(solution)/shard_map/reduce_scatter | solution.py:155
  612.8 2.5 add_convert_fusion
  (96 shorter events, 24.1 us)
Async XLA Ops:
  6.5 42.8 %copy-start.4 = (f32[2048]{0:T(1024)S(1)}, f32[2048]{0:T(1024)}, u32[]{:S(2)}) copy-start(f32[2048]{0:T(1024)} %param.17) | copy-start | bytes 24580
  6.5 39.6 %all-gather.9.cloned.1.call-start = ((), (), s32[]{:S(2)}) async-start(), calls=%async_computation.2 | async-start | bytes 5242880 | tf_op jit(solution)/shard_map/all_gather | solution.py:94
  7.3 68.4 %all-gather.11.cloned.1.call-start = ((), (), s32[]{:S(2)}) async-start(), calls=%async_computation.3 | async-start | bytes 1310720 | tf_op jit(solution)/shard_map/all_gather | solution.py:100
  8.0 96.7 %all-gather.13.cloned.1.call-start = ((), (), s32[]{:S(2)}) async-start(), calls=%async_computation.4 | async-start | bytes 1310720 | tf_op jit(solution)/shard_map/all_gather | solution.py:101
  8.7 124.8 %all-gather.15.cloned.1.call-start = ((), (), s32[]{:S(2)}) async-start(), calls=%async_computation.5 | async-start | bytes 1310720 | tf_op jit(solution)/shard_map/all_gather | solution.py:134
  9.3 181.3 %reduce-scatter.3.cloned.1.call-start = ((), (), s32[]{:S(2)}) async-start(), calls=%async_computation.6 | async-start | bytes 5242880 | tf_op jit(solution)/shard_map/reduce_scatter | solution.py:137
  46.1 3.4 copy-start.1
  50.6 1.9 copy-start
  99.1 37.7 %copy-start.6 = (f32[2,128]{1,0:T(2,128)S(1)}, f32[2,128]{1,0:T(2,128)}, u32[]{:S(2)}) copy-start(f32[2,128]{1,0:T(2,128)} %param.23) | copy-start | bytes 3076
  136.8 53.9 %copy-start.3 = (bf16[1024,512]{1,0:T(8,128)(2,1)S(1)}, bf16[1024,512]{1,0:T(8,128)(2,1)}, u32[]{:S(2)}) copy-start(bf16[1024,512]{1,0:T(8,128)(2,1)} %param.16) | copy-start | bytes 3145732
  146.7 189.3 %copy-start.5 = (f32[2048]{0:T(1024)S(1)}, f32[2048]{0:T(1024)}, u32[]{:S(2)}) copy-start(f32[2048]{0:T(1024)} %param.24) | copy-start | bytes 24580
  146.7 81.0 %all-gather.17.cloned.1.call-start = ((), (), s32[]{:S(2)}) async-start(), calls=%async_computation.7 | async-start | bytes 5242880 | tf_op jit(solution)/shard_map/all_gather | solution.py:141
  193.1 142.9 %all-gather.19.cloned.1.call-start = ((), (), s32[]{:S(2)}) async-start(), calls=%async_computation.8 | async-start | bytes 7208960 | tf_op jit(solution)/shard_map/all_gather | solution.py:147
  193.9 248.7 %all-gather.21.cloned.1.call-start = ((), (), s32[]{:S(2)}) async-start(), calls=%async_computation.9 | async-start | bytes 7208960 | tf_op jit(solution)/shard_map/all_gather | solution.py:148
  194.6 354.5 %all-gather.23.cloned.1.call-start = ((), (), s32[]{:S(2)}) async-start(), calls=%async_computation.10 | async-start | bytes 7208960 | tf_op jit(solution)/shard_map/all_gather | solution.py:152
  195.4 417.5 %reduce-scatter.5.cloned.1.call-start = ((), (), s32[]{:S(2)}) async-start(), calls=%async_computation.11 | async-start | bytes 5242880 | tf_op jit(solution)/shard_map/reduce_scatter | solution.py:155
  347.9 264.9 %copy-start.2 = (bf16[1024,512]{1,0:T(8,128)(2,1)S(1)}, bf16[1024,512]{1,0:T(8,128)(2,1)}, u32[]{:S(2)}) copy-start(bf16[1024,512]{1,0:T(8,128)(2,1)} %add_convert_fusion.1) | copy-start | bytes 3145732
Sparse Core Ops, SparseCore 0:
  8.9 37.1 all-gather.8
  47.7 27.9 all-gather.10
  77.3 27.3 all-gather.12
  106.1 27.3 all-gather.14
  146.8 43.7 reduce-scatter.2
  193.2 34.4 all-gather.16
  229.3 106.6 all-gather.18
  337.6 104.9 all-gather.20
  444.1 104.9 all-gather.22
  570.1 42.6 reduce-scatter.4
where the time goes:
time: 623 us; the launch traced here: 622 us
  waiting for transfers between devices  473 us (76%)
  matrix products  60 us (10%)
  blocking collectives  34.1 us (5%)
  local copies, waits for them, and re-layouts  22.2 us (4%)
  other arithmetic  18.5 us (3%)
  between operations  13.7 us (2%)
    all_gather x1, waiting for transfers between devices, per_device(): lax.all_gather(ffn_down, 'fs', axis=1, tiled=True)  107 us
    all_gather x1, waiting for transfers between devices, per_device(): gate_hidden = add_rows(lax.all_gather(ffn_gate, 'fs', axis=0, tiled=True))  105 us
    all_gather x1, waiting for transfers between devices, per_device(): up_hidden = add_rows(lax.all_gather(ffn_up, 'fs', axis=0, tiled=True))  94.7 us
    reduce_scatter x1, waiting for transfers between devices, per_device(): lax.psum_scatter(mixer_terms.astype(jnp.bfloat16), 'tp', scatter_dimensio...  43.9 us
    reduce_scatter x1, waiting for transfers between devices, per_device(): lax.psum_scatter(ffn_terms.astype(jnp.bfloat16), 'tp', scatter_dimension=...  42.8 us
    all_gather x1, waiting for transfers between devices, per_device(): resid_whole = lax.all_gather(resid_shard, 'tp', axis=1, tiled=True)  32.3 us
    all_gather x1, waiting for transfers between devices, per_device(): lax.all_gather(out_weight, 'fs', axis=1, tiled=True)  28.8 us
    dot_general x1, matrix products, per_device(): jnp.dot(hidden, lax.all_gather(ffn_down, 'fs', axis=1, tiled=True), prefe...  20.9 us
  transfers between devices with their start and end apart: 10, of which 10 were waited for; matrix products, arithmetic and copies ran while one was open for 10% of the time, Pallas kernels for 0%

commit v1 on v0

--- a/solution.py
+++ b/solution.py
@@ -145,7 +145,14 @@
         return jnp.dot(normed_ffn, weight_piece, preferred_element_type=jnp.float32)
 
     gate_hidden = add_rows(lax.all_gather(ffn_gate, "fs", axis=0, tiled=True))
-    up_hidden = add_rows(lax.all_gather(ffn_up, "fs", axis=0, tiled=True))
+    up_hidden = add_rows(
+        jnp.concatenate(
+            jax.lax.all_to_all(
+                jnp.stack([ffn_up for _ in range(jax.lax.psum(1, "fs"))], axis=0), "fs", 0, 0
+            ),
+            axis=0,
+        )
+    )
     hidden = (jax.nn.silu(gate_hidden) * up_hidden).astype(jnp.bfloat16)
     ffn_terms = jnp.dot(
         hidden,

time: 623 us -> 602 us (0.966)
  waiting for transfers between devices: 473 us -> 444 us
    all_gather x1 -> x0, waiting for transfers between devices: 94.7 us -> none  [per_device(): up_hidden = add_rows(lax.all_gather(ffn_up, 'fs', axis=0, tiled=True))]
    all_gather x1, waiting for transfers between devices: 105 us -> 182 us  [per_device(): gate_hidden = add_rows(lax.all_gather(ffn_gate, 'fs', axis=0, tiled=True))]
    all_gather x1, waiting for transfers between devices: 32.3 us -> 24.7 us  [per_device(): resid_whole = lax.all_gather(resid_shard, 'tp', axis=1, tiled=True)]
  transfers between devices with their start and end apart: 10 -> 10, of which waited for: 10 -> 9; matrix products, arithmetic and copies ran while one was open for 10% -> 10% of each run, Pallas kernels for 0% -> 0%
where the time goes in v1:
time: 602 us; the launch traced here: 601 us
  waiting for transfers between devices  444 us (74%)
  matrix products  60.1 us (10%)
  blocking collectives  34.1 us (6%)
  local copies, waits for them, and re-layouts  25.1 us (4%)
  other arithmetic  18.5 us (3%)
  between operations  13.4 us (2%)
    all_gather x1, waiting for transfers between devices, per_device(): gate_hidden = add_rows(lax.all_gather(ffn_gate, 'fs', axis=0, tiled=True))  182 us
    all_gather x1, waiting for transfers between devices, per_device(): lax.all_gather(ffn_down, 'fs', axis=1, tiled=True)  104 us
    reduce_scatter x1, waiting for transfers between devices, per_device(): lax.psum_scatter(mixer_terms.astype(jnp.bfloat16), 'tp', scatter_dimensio...  43.9 us
    reduce_scatter x1, waiting for transfers between devices, per_device(): lax.psum_scatter(ffn_terms.astype(jnp.bfloat16), 'tp', scatter_dimension=...  42.8 us
    all_gather x1, waiting for transfers between devices, per_device(): lax.all_gather(out_weight, 'fs', axis=1, tiled=True)  28.8 us
    all_gather x1, waiting for transfers between devices, per_device(): resid_whole = lax.all_gather(resid_shard, 'tp', axis=1, tiled=True)  24.7 us
    dot_general x1, matrix products, per_device(): jnp.dot(hidden, lax.all_gather(ffn_down, 'fs', axis=1, tiled=True), prefe...  21 us
    all_gather x1, blocking collectives, per_device(): lax.all_gather(key_weight, 'fs', axis=0, tiled=True)  17.6 us
  transfers between devices with their start and end apart: 10, of which 9 were waited for; matrix products, arithmetic and copies ran while one was open for 10% of the time, Pallas kernels for 0%

profile of v1, /device:TPU:0, one launch (start us, length us, event | category | flops | bytes accessed | tf_op | source)
XLA Modules:
  0.0 601.4 jit_solution(747601244638357048)
XLA Ops:
  9.5 17.6 %all_gather.28 = bf16[2048,128]{1,0:T(8,128)(2,1)S(1)} all-gather(bf16[512,128]{1,0:T(8,128)(2,1)} %param.19), channel_id=1, replica_groups=mesh['rep'=2,'fs'=4,'tp'=4] {'fs'}, dimensions={0}, use_global_device_ids=true | all-gather | bytes 655360 | tf_op jit(solution)/shard_map/all_gather | solution.py:99
  27.0 16.6 %all_gather.30 = bf16[2048,128]{1,0:T(8,128)(2,1)S(1)} all-gather(bf16[512,128]{1,0:T(8,128)(2,1)} %param.18), channel_id=1, replica_groups=mesh['rep'=2,'fs'=4,'tp'=4] {'fs'}, dimensions={0}, use_global_device_ids=true | all-gather | bytes 655360 | tf_op jit(solution)/shard_map/all_gather | solution.py:98
  46.1 3.2 fusion.25
  50.6 1.9 copy-done
  54.4 3.9 fusion.35
  58.5 2.1 multiply_subtract_fusion
  61.6 1.8 mul.286
  63.4 1.9 reshape_reshape.24
  65.3 10.4 %all-gather.10.cloned.1.call-done = bf16[2048,256]{1,0:T(8,128)(2,1)} async-done(((bf16[512,256]{1,0:T(8,128)(2,1)}), bf16[2048,256]{1,0:T(8,128)(2,1)}) %all-gather.10.cloned.1.call-update) | async-done | bytes 1048592 | tf_op jit(solution)/shard_map/all_gather | solution.py:100
  75.7 3.7 fusion.31
  80.1 19.0 %while.15 = (s32[]{:T(128)}, f32[4,2,64,128]{3,2,1,0:T(8,128)S(1)}, f32[4,4,64,2,128]{4,2,3,1,0:T(8,128)S(1)}, f32[4,4,64,2,64]{2,0,1,4,3:T(4,128)}, f32[4,4,64,...) while((s32[]{:T(128)}, f32[4,2,64,128]{3,2,1,0:T(8,128)S(1)}, ...), condition=%wide.region_2.4_spmd.clone.clone.clone, body=%wide.region_1.3_spmd.clone.clone.clone.sunk | while | flops 176603408 | bytes 4415676 | solution.py:74
  80.3 2.1 constant_dynamic-slice_fusion.3
  85.0 2.1 constant_dynamic-slice_fusion.3
  89.7 2.1 constant_dynamic-slice_fusion.3
  94.4 2.1 constant_dynamic-slice_fusion.3
  100.7 1.8 copy.35
  102.5 2.2 all-gather.12.cloned.1.call-done
  104.7 28.8 %all-gather.14.cloned.1.call-done = bf16[256,2048]{1,0:T(8,128)(2,1)} async-done(((bf16[256,512]{1,0:T(8,128)(2,1)}), bf16[256,2048]{1,0:T(8,128)(2,1)}) %all-gather.14.cloned.1.call-update) | async-done | bytes 1048592 | tf_op jit(solution)/shard_map/all_gather | solution.py:134
  134.7 2.0 sub.86
  136.8 9.9 %convolution_convert_fusion.1 = bf16[1024,2048]{1,0:T(8,128)(2,1)} fusion(bf16[256,2048]{1,0:T(8,128)(2,1)} %all-gather.14.cloned.1.call-done, bf16[1024,2048]{1,0:T(8,128)(2,1)} %copy-done, bf16[2048,256]{1,0:T(8,128)(2,1)} %all-gather.12.cloned.1.call-done, f32[128,8,2,128]{3,2,1,0:T(2,128)S(1)} %bitcast.115, f32[128,8,2,128]{3,2,1,0:T(2,128)} %bitcast.116, ...), kind=kOutput, calls=%fused_computation.45 | convolution fusion | flops 2152464384 | bytes 13632512 | tf_op jit(solution)/shard_map/dot_general | solution.py:132
  146.8 43.9 %reduce-scatter.3.cloned.1.call-done = bf16[1024,512]{1,0:T(8,128)(2,1)} async-done(((bf16[1024,2048]{1,0:T(8,128)(2,1)}), bf16[1024,512]{1,0:T(8,128)(2,1)}) %reduce-scatter.3.cloned.1.call-update) | async-done | bytes 1048592 | tf_op jit(solution)/shard_map/reduce_scatter | solution.py:137
  190.6 2.5 add_convert_fusion.1
  193.9 2.9 stack.8
  196.8 5.4 all-to-all-start
  203.0 24.7 %all-gather.16.cloned.1.call-done = bf16[1024,2048]{1,0:T(8,128)(2,1)} async-done(((bf16[1024,512]{1,0:T(8,128)(2,1)}), bf16[1024,2048]{1,0:T(8,128)(2,1)}) %all-gather.16.cloned.1.call-update) | async-done | bytes 4194320 | tf_op jit(solution)/shard_map/all_gather | solution.py:141
  227.7 3.1 fusion.28
  230.8 182.0 %all-gather.18.cloned.1.call-done = bf16[2048,1408]{1,0:T(8,128)(2,1)} async-done(((bf16[512,1408]{1,0:T(8,128)(2,1)}), bf16[2048,1408]{1,0:T(8,128)(2,1)}) %all-gather.18.cloned.1.call-update) | async-done | bytes 5767184 | tf_op jit(solution)/shard_map/all_gather | solution.py:147
  412.8 11.9 %fusion.33 = f32[1024,1408]{1,0:T(8,128)} fusion(bf16[2048,1408]{1,0:T(8,128)(2,1)} %all-gather.18.cloned.1.call-done, bf16[1024,2048]{1,0:T(8,128)(2,1)} %all-gather.16.cloned.1.call-done, f32[2048]{0:T(1024)S(1)} %copy-done.6, f32[1024]{0:T(1024)S(1)} %add_rsqrt_fusion), kind=kOutput, calls=%fused_computation.53 | convolution fusion | flops 5913968640 | bytes 15740928 | tf_op jit(solution)/shard_map/dot_general | solution.py:145
  424.7 103.9 %all-gather.20.cloned.1.call-done = bf16[1408,2048]{1,0:T(8,128)(2,1)} async-done(((bf16[1408,512]{1,0:T(8,128)(2,1)}), bf16[1408,2048]{1,0:T(8,128)(2,1)}) %all-gather.20.cloned.1.call-update) | async-done | bytes 5767184 | tf_op jit(solution)/shard_map/all_gather | solution.py:159
  528.6 21.0 %convolution_convert_fusion = bf16[1024,2048]{1,0:T(8,128)(2,1)} fusion(bf16[1408,2048]{1,0:T(8,128)(2,1)} %all-gather.20.cloned.1.call-done, f32[1024,1408]{1,0:T(8,128)} %fusion.33, bf16[2048,1408]{1,0:T(8,128)(2,1)} %bitcast.8, bf16[1024,2048]{1,0:T(8,128)(2,1)} %all-gather.16.cloned.1.call-done, f32[2048]{0:T(1024)S(1)} %copy-done.6, ...), kind=kOutput, calls=%fused_computation.44 | convolution fusion | flops 11830296576 | bytes 25702400 | tf_op jit(solution)/shard_map/dot_general | solution.py:157
  549.6 42.8 %reduce-scatter.5.cloned.1.call-done = bf16[1024,512]{1,0:T(8,128)(2,1)} async-done(((bf16[1024,2048]{1,0:T(8,128)(2,1)}), bf16[1024,512]{1,0:T(8,128)(2,1)}) %reduce-scatter.5.cloned.1.call-update) | async-done | bytes 1048592 | tf_op jit(solution)/shard_map/reduce_scatter | solution.py:162
  592.4 2.5 add_convert_fusion
  (98 shorter events, 24.9 us)
Async XLA Ops:
  6.5 42.8 %copy-start.5 = (f32[2048]{0:T(1024)S(1)}, f32[2048]{0:T(1024)}, u32[]{:S(2)}) copy-start(f32[2048]{0:T(1024)} %param.17) | copy-start | bytes 24580
  6.5 39.6 %all-gather.8.cloned.1.call-start = ((), (), s32[]{:S(2)}) async-start(), calls=%async_computation.3 | async-start | bytes 5242880 | tf_op jit(solution)/shard_map/all_gather | solution.py:94
  7.3 68.4 %all-gather.10.cloned.1.call-start = ((), (), s32[]{:S(2)}) async-start(), calls=%async_computation.4 | async-start | bytes 1310720 | tf_op jit(solution)/shard_map/all_gather | solution.py:100
  8.0 96.7 %all-gather.12.cloned.1.call-start = ((), (), s32[]{:S(2)}) async-start(), calls=%async_computation.5 | async-start | bytes 1310720 | tf_op jit(solution)/shard_map/all_gather | solution.py:101
  8.7 124.8 %all-gather.14.cloned.1.call-start = ((), (), s32[]{:S(2)}) async-start(), calls=%async_computation.6 | async-start | bytes 1310720 | tf_op jit(solution)/shard_map/all_gather | solution.py:134
  9.3 181.3 %reduce-scatter.3.cloned.1.call-start = ((), (), s32[]{:S(2)}) async-start(), calls=%async_computation.7 | async-start | bytes 5242880 | tf_op jit(solution)/shard_map/reduce_scatter | solution.py:137
  46.1 3.4 copy-start.1
  50.6 1.9 copy-start
  99.1 37.7 %copy-start.7 = (f32[2,128]{1,0:T(2,128)S(1)}, f32[2,128]{1,0:T(2,128)}, u32[]{:S(2)}) copy-start(f32[2,128]{1,0:T(2,128)} %param.23) | copy-start | bytes 3076
  136.8 53.9 %copy-start.3 = (bf16[1024,512]{1,0:T(8,128)(2,1)S(1)}, bf16[1024,512]{1,0:T(8,128)(2,1)}, u32[]{:S(2)}) copy-start(bf16[1024,512]{1,0:T(8,128)(2,1)} %param.16) | copy-start | bytes 3145732
  146.7 47.2 %copy-start.4 = (bf16[512,1408]{1,0:T(8,128)(2,1)S(1)}, bf16[512,1408]{1,0:T(8,128)(2,1)}, u32[]{:S(2)}) copy-start(bf16[512,1408]{1,0:T(8,128)(2,1)} %param.26) | copy-start | bytes 4325380
  146.7 81.0 %all-gather.16.cloned.1.call-start = ((), (), s32[]{:S(2)}) async-start(), calls=%async_computation.8 | async-start | bytes 5242880 | tf_op jit(solution)/shard_map/all_gather | solution.py:141
  193.1 219.7 %all-gather.18.cloned.1.call-start = ((), (), s32[]{:S(2)}) async-start(), calls=%async_computation.9 | async-start | bytes 7208960 | tf_op jit(solution)/shard_map/all_gather | solution.py:147
  196.8 216.1 %copy-start.6 = (f32[2048]{0:T(1024)S(1)}, f32[2048]{0:T(1024)}, u32[]{:S(2)}) copy-start(f32[2048]{0:T(1024)} %param.24) | copy-start | bytes 24580
  196.8 228.0 %all-to-all-start = ((bf16[4,512,1408]{2,1,0:T(8,128)(2,1)}), bf16[4,512,1408]{2,1,0:T(8,128)(2,1)}, u32[]{:S(2)}, u32[]{:S(2)}) async-start(bf16[4,512,1408]{2,1,0:T(8,128)(2,1)} %stack.8), calls=%async_computation.1 | async-start | bytes 11534336 | tf_op jit(solution)/shard_map/all_to_all | solution.py:150
  202.2 326.4 %all-gather.20.cloned.1.call-start = ((), (), s32[]{:S(2)}) async-start(), calls=%async_computation.10 | async-start | bytes 7208960 | tf_op jit(solution)/shard_map/all_gather | solution.py:159
  202.9 389.4 %reduce-scatter.5.cloned.1.call-start = ((), (), s32[]{:S(2)}) async-start(), calls=%async_computation.11 | async-start | bytes 5242880 | tf_op jit(solution)/shard_map/reduce_scatter | solution.py:162
  528.6 63.8 %copy-start.2 = (bf16[1024,512]{1,0:T(8,128)(2,1)S(1)}, bf16[1024,512]{1,0:T(8,128)(2,1)}, u32[]{:S(2)}) copy-start(bf16[1024,512]{1,0:T(8,128)(2,1)} %add_convert_fusion.1) | copy-start | bytes 3145732
Sparse Core Ops, SparseCore 0:
  8.9 37.1 all-gather.7
  47.7 27.9 all-gather.9
  77.3 27.3 all-gather.11
  106.1 27.3 all-gather.13
  146.8 43.7 reduce-scatter.2
  193.2 34.4 all-gather.15
  229.3 183.4 all-gather.17
  414.4 114.1 all-gather.19
  549.7 42.6 reduce-scatter.4
